TPU v7x, 32 devices: a whole 2x2x4 slice. The times are simulated.
32 devices in a mesh: kv: 8 (over z, y), tp: 4 (over x, core).
Axes of the slice: x: 2, y: 2, z: 4, core: 2. Of those that a mesh axis runs over, the one named last changes fastest.
Arguments:
- residual_in: bfloat16 [64, 2048], P(None, ('kv', 'tp')), may hold values from -14 to 14
- delta_state: float32 [64, 32, 128, 128], P('kv', 'tp'), may hold values from -1 to 1
- norm_gain_first: float32 [2048], P('kv'), may hold values from 0.1 to 1.9
- gate_first: bfloat16 [2048, 5632], P('kv', 'tp'), may hold values from -0.125 to 0.125
- up_first: bfloat16 [2048, 5632], P('kv', 'tp'), may hold values from -0.125 to 0.125
- down_first: bfloat16 [5632, 2048], P('tp', 'kv'), may hold values from -0.15625 to 0.15625
- norm_gain_mixer: float32 [2048], P('kv'), may hold values from 0.1 to 1.9
- query_weight: bfloat16 [2048, 2048], P('kv', 'tp'), may hold values from -0.125 to 0.125
- key_weight: bfloat16 [2048, 2048], P('kv', 'tp'), may hold values from -0.125 to 0.125
- value_weight: bfloat16 [2048, 4096], P('kv', 'tp'), may hold values from -0.125 to 0.125
- output_gate_weight: bfloat16 [2048, 4096], P('kv', 'tp'), may hold values from -0.125 to 0.125
- beta_weight: bfloat16 [2048, 32], P('kv'), may hold values from -0.125 to 0.125
- decay_weight: bfloat16 [2048, 32], P('kv'), may hold values from -0.125 to 0.125
- decay_rate: float32 [32], P('tp'), may hold values from -2.3 to 1.1
- decay_bias: float32 [32], P('tp'), may hold values from -1 to 1
- head_gain: float32 [128], replicated, may hold values from 0.1 to 1.9
- out_weight: bfloat16 [4096, 2048], P('tp', 'kv'), may hold values from -0.125 to 0.125
- norm_gain_second: float32 [2048], P('kv'), may hold values from 0.1 to 1.9
- gate_second: bfloat16 [2048, 5632], P('kv', 'tp'), may hold values from -0.125 to 0.125
- up_second: bfloat16 [2048, 5632], P('kv', 'tp'), may hold values from -0.125 to 0.125
- down_second: bfloat16 [5632, 2048], P('tp', 'kv'), may hold values from -0.15625 to 0.15625
Outputs:
- residual_out: bfloat16 [64, 2048], P(None, ('kv', 'tp'))
- delta_state_out: float32 [64, 32, 128, 128], P('kv', 'tp')
All inputs are finite; a program needn't handle non-finite values.
Results may differ from a plain program's by a relative error of at most 0.03.
Values may be sent and summed in bfloat16 or wider, within the bound.
A program may use at most 64 MiB of HBM per device.

v0:
```python
import jax
import jax.numpy as jnp
from jax import lax
from jax.sharding import PartitionSpec as P

D = 2048
epsilon = 1e-06


def activate(summed, square_sums, hidden_cols):
    rowscale = lax.rsqrt(square_sums / D + epsilon)[:, None]
    gate_act = summed[:, :hidden_cols] * rowscale
    up_act = summed[:, hidden_cols:] * rowscale
    return (jax.nn.silu(gate_act) * up_act).astype(jnp.bfloat16)


def feed_forward(residual, norm_gain, gate_weight, up_weight, down_weight, finish):
    as_float = residual.astype(jnp.float32)
    squares = jnp.sum(as_float * as_float, axis=1)
    scaled = (as_float * norm_gain).astype(jnp.bfloat16)
    joined = jnp.concatenate([gate_weight, up_weight], axis=1)
    partial_value = jnp.dot(scaled, joined, preferred_element_type=jnp.float32)
    hidden_cols = gate_weight.shape[1]
    summed, square_sums = (
        lax.psum(partial_value.astype(jnp.bfloat16), "kv").astype(jnp.float32),
        lax.psum(squares.astype(jnp.bfloat16), "kv").astype(jnp.float32),
    )
    hidden = activate(summed, square_sums, hidden_cols)
    projected = jnp.dot(hidden, down_weight, preferred_element_type=jnp.float32).astype(
        jnp.bfloat16
    )
    if finish:
        col_count = residual.shape[1] // lax.axis_size("tp")
        own_cols = lax.dynamic_slice_in_dim(
            as_float, lax.axis_index("tp") * col_count, col_count, 1
        )
        branch = lax.psum_scatter(projected, "tp", scatter_dimension=1, tiled=True).astype(
            jnp.float32
        )
        return (own_cols + 0.5 * branch).astype(jnp.bfloat16)
    branch = lax.psum(projected, "tp").astype(jnp.float32)
    return (as_float + 0.5 * branch).astype(jnp.bfloat16)


def unit_heads(projected, head_size):
    activated = jax.nn.silu(projected).reshape(projected.shape[0], -1, head_size)
    return activated * lax.rsqrt(jnp.sum(activated * activated, axis=-1, keepdims=True) + epsilon)


def delta_step(old_state, key_rows, queries, values, beta_gate, decay_gate):
    faded_state = old_state * decay_gate[:, :, None, None]
    predicted = jnp.einsum("rhab,rha->rhb", faded_state, key_rows, precision=lax.Precision.HIGHEST)
    correction = beta_gate[:, :, None] * (values - predicted)
    updated = faded_state + key_rows[:, :, :, None] * correction[:, :, None, :]
    reading = jnp.einsum("rhab,rha->rhb", updated, queries, precision=lax.Precision.HIGHEST)
    return (updated, reading)


def token_mixer(
    residual,
    norm_gain,
    query_weight,
    key_weight,
    value_weight,
    output_gate_weight,
    beta_weight,
    decay_weight,
    decay_rate,
    decay_bias,
    head_gain,
    out_weight,
    old_state,
):
    as_float = residual.astype(jnp.float32)
    squares = jnp.sum(as_float * as_float, axis=1)
    scaled = (as_float * norm_gain).astype(jnp.bfloat16)
    joined = jnp.concatenate([query_weight, key_weight, value_weight, output_gate_weight], axis=1)
    partial_value = jnp.dot(scaled, joined, preferred_element_type=jnp.float32)
    heads_dev = decay_rate.shape[0]
    head_start = lax.axis_index("tp") * heads_dev
    gate_cols = jnp.concatenate(
        [
            lax.dynamic_slice_in_dim(beta_weight, head_start, heads_dev, 1),
            lax.dynamic_slice_in_dim(decay_weight, head_start, heads_dev, 1),
        ],
        axis=1,
    )
    gate_part = jnp.dot(scaled, gate_cols, preferred_element_type=jnp.float32)
    row_count = old_state.shape[0]
    square_sums = lax.psum(squares, "kv")
    square_sums = lax.dynamic_slice_in_dim(
        square_sums, lax.axis_index("kv") * row_count, row_count, 0
    )
    summed, gate_summed = (
        lax.psum_scatter(
            partial_value.astype(jnp.bfloat16), "kv", scatter_dimension=0, tiled=True
        ).astype(jnp.float32),
        lax.psum_scatter(
            gate_part.astype(jnp.bfloat16), "kv", scatter_dimension=0, tiled=True
        ).astype(jnp.float32),
    )
    rowscale = lax.rsqrt(square_sums / D + epsilon)[:, None]
    summed = summed * rowscale
    gate_summed = gate_summed * rowscale
    head_size = old_state.shape[2]
    key_cols = query_weight.shape[1]
    value_cols = value_weight.shape[1]
    repeat_count = heads_dev // (key_cols // head_size)
    queries = jnp.repeat(
        unit_heads(summed[:, :key_cols], head_size) * head_size ** (-0.5), repeat_count, axis=1
    )
    key_rows = jnp.repeat(
        unit_heads(summed[:, key_cols : 2 * key_cols], head_size), repeat_count, axis=1
    )
    values = jax.nn.silu(summed[:, 2 * key_cols : 2 * key_cols + value_cols]).reshape(
        row_count, heads_dev, head_size
    )
    out_gate = jax.nn.silu(summed[:, 2 * key_cols + value_cols :]).reshape(
        row_count, heads_dev, head_size
    )
    beta_gate = jax.nn.sigmoid(gate_summed[:, :heads_dev])
    decay_gate = jnp.exp(
        -jnp.exp(decay_rate)[None, :]
        * jax.nn.softplus(gate_summed[:, heads_dev:] + decay_bias[None, :])
    )
    new_state, reading = delta_step(old_state, key_rows, queries, values, beta_gate, decay_gate)
    normed = reading * lax.rsqrt(jnp.mean(reading * reading, axis=-1, keepdims=True) + epsilon)
    normed = (
        (normed * head_gain * out_gate)
        .reshape(row_count, heads_dev * head_size)
        .astype(jnp.bfloat16)
    )
    projected = jnp.dot(
        lax.all_gather(normed, "kv", axis=0, tiled=True),
        out_weight,
        preferred_element_type=jnp.float32,
    ).astype(jnp.bfloat16)
    branch = lax.psum(projected, "tp").astype(jnp.float32)
    return ((as_float + branch).astype(jnp.bfloat16), new_state)


def body(
    residual_in,
    delta_state,
    norm_gain_first,
    gate_first,
    up_first,
    down_first,
    norm_gain_mixer,
    query_weight,
    key_weight,
    value_weight,
    output_gate_weight,
    beta_weight,
    decay_weight,
    decay_rate,
    decay_bias,
    head_gain,
    out_weight,
    norm_gain_second,
    gate_second,
    up_second,
    down_second,
):
    columns = lax.all_gather(residual_in, "tp", axis=1, tiled=True)
    after_first = feed_forward(columns, norm_gain_first, gate_first, up_first, down_first, False)
    after_mixer, new_state = token_mixer(
        after_first,
        norm_gain_mixer,
        query_weight,
        key_weight,
        value_weight,
        output_gate_weight,
        beta_weight,
        decay_weight,
        decay_rate,
        decay_bias,
        head_gain,
        out_weight,
        delta_state,
    )
    residual_out = feed_forward(
        after_mixer, norm_gain_second, gate_second, up_second, down_second, True
    )
    return (residual_out, new_state)


def solution(mesh):
    placed = (
        P(None, ("kv", "tp")),
        P("kv", "tp", None, None),
        P("kv"),
        P("kv", "tp"),
        P("kv", "tp"),
        P("tp", "kv"),
        P("kv"),
        P("kv", "tp"),
        P("kv", "tp"),
        P("kv", "tp"),
        P("kv", "tp"),
        P("kv", None),
        P("kv", None),
        P("tp"),
        P("tp"),
        P(),
        P("tp", "kv"),
        P("kv"),
        P("kv", "tp"),
        P("kv", "tp"),
        P("tp", "kv"),
    )
    return jax.shard_map(
        body,
        mesh=mesh,
        in_specs=placed,
        out_specs=(P(None, ("kv", "tp")), P("kv", "tp", None, None)),
        check_vma=False,
    )
```

profile of v0, /device:TPU:0, one launch (start us, length us, event | category | flops | bytes accessed | tf_op | source)
XLA Modules:
  0.0 322.3 jit_solution(16253293188831210375)
XLA Ops:
  7.2 0.9 copy.27
  8.1 6.2 %all_gather.6 = bf16[64,256]{0,1:T(8,128)(2,1)S(1)} all-gather(bf16[64,64]{0,1:T(8,128)(2,1)S(1)} %copy.27), channel_id=1, replica_groups=mesh['kv'=8,'tp'=4] {'tp'}, dimensions={1}, use_global_device_ids=true | all-gather | bytes 40960 | tf_op jit(solution)/shard_map/all_gather | solution.py:165
  14.3 0.1 copy.28
  14.4 2.6 convolution_convert_fusion.2
  17.0 0.0 reduce-scatter.5.cloned.1.call-start
  17.1 0.1 fusion.27
  17.2 22.4 %psum.50 = bf16[64]{0:T(256)(128)(2,1)S(1)} all-reduce(bf16[64]{0:T(256)(128)(2,1)S(1)} %fusion.27), channel_id=1, replica_groups=mesh['kv'=8,'tp'=4] {'kv'}, use_global_device_ids=true, to_apply=%region_2.0 | all-reduce | flops 64 | bytes 256 | tf_op jit(solution)/shard_map/psum | solution.py:26
  39.6 1.2 dynamic-slice
  41.5 0.7 constant_dynamic-slice_fusion
  42.2 0.7 exponential_negate_fusion
  42.9 47.6 %all-reduce.4.cloned.1.call-done = bf16[64,2816]{1,0:T(8,128)(2,1)} async-done(((bf16[64,2816]{1,0:T(8,128)(2,1)}), bf16[64,2816]{1,0:T(8,128)(2,1)}) %all-reduce.4.cloned.1.call-update) | async-done | bytes 360464 | tf_op jit(solution)/shard_map/psum | solution.py:25
  90.5 1.0 convert_element_type.96
  91.5 0.3 convolution_convert_fusion.5
  91.9 10.3 %psum.51 = bf16[64,256]{1,0:T(8,128)(2,1)S(1)} all-reduce(bf16[64,256]{1,0:T(8,128)(2,1)S(1)} %convolution_convert_fusion.5), channel_id=1, replica_groups=mesh['kv'=8,'tp'=4] {'tp'}, use_global_device_ids=true, to_apply=%region_3.4 | all-reduce | flops 16384 | bytes 65536 | tf_op jit(solution)/shard_map/psum | solution.py:41
  102.1 0.1 fusion.30
  102.3 1.1 convolution_convert_fusion.1
  103.5 0.0 all-reduce.6.cloned.1.call-start
  103.5 19.7 %psum.52 = f32[64]{0:T(128)S(1)} all-reduce(f32[64]{0:T(128)S(1)} %get-tuple-element.4), channel_id=1, replica_groups=mesh['kv'=8,'tp'=4] {'kv'}, use_global_device_ids=true, to_apply=%region_6.7 | all-reduce | flops 64 | bytes 512 | tf_op jit(solution)/shard_map/psum | solution.py:90
  123.3 0.1 convolution_convert_fusion.6
  123.4 33.1 %all-reduce = bf16[64,16]{1,0:T(8,128)(2,1)S(1)} all-reduce(bf16[64,16]{1,0:T(8,128)(2,1)S(1)} %convolution_convert_fusion.6), channel_id=2, replica_groups=mesh['kv'=8,'tp'=4] {'kv'}, use_global_device_ids=true, to_apply=%region_4.5.clone | all-reduce | flops 1024 | bytes 4096
  156.5 0.1 add_rsqrt_fusion.4
  156.5 0.1 convert_multiply_fusion.5
  156.6 0.1 add_divide_fusion
  156.7 0.1 copy.30
  156.8 8.5 %reduce-scatter.5.cloned.1.call-done = bf16[8,3072]{1,0:T(8,128)(2,1)} async-done(((bf16[64,3072]{1,0:T(8,128)(2,1)}), bf16[8,3072]{1,0:T(8,128)(2,1)}) %reduce-scatter.5.cloned.1.call-update) | async-done | bytes 49168 | tf_op jit(solution)/shard_map/reduce_scatter | solution.py:95
  165.2 1.0 convert_multiply_fusion
  166.3 0.1 fusion.42
  166.4 0.1 fusion.43
  166.5 5.8 %fusion = f32[8,8,1,128]{3,2,1,0:T(1,128)S(1)} fusion(f32[8,8,128,1]{2,3,1,0:T(1,128)S(1)} %bitcast.57, f32[8,8,128,128]{3,2,1,0:T(8,128)} %param.22, f32[8,8]{1,0:T(8,128)S(1)} %get-tuple-element.11), kind=kOutput, calls=%fused_computation.1 | convolution fusion | flops 13631488 | bytes 4260096 | tf_op jit(solution)/shard_map/rhab,rha->rhb/dot_general | solution.py:52
  172.3 0.1 fusion.37
  172.4 1.5 multiply_add_fusion
  174.0 2.0 copy-done.2
  176.0 3.6 %fusion.59 = f32[8,8,1,128]{3,2,1,0:T(1,128)S(1)} fusion(f32[8,8,128,128]{3,2,1,0:T(8,128)S(1)} %multiply_add_fusion, f32[8,8,128,1]{2,3,1,0:T(1,128)S(1)} %bitcast.60), kind=kOutput, calls=%fused_computation.96 | convolution fusion | flops 12582912 | bytes 4259840 | tf_op jit(solution)/shard_map/rhab,rha->rhb/dot_general | solution.py:55
  179.7 0.1 fusion.35
  179.8 0.1 fusion.45
  179.9 30.6 %all_gather.7 = bf16[64,1024]{1,0:T(8,128)(2,1)S(1)} all-gather(bf16[8,1024]{1,0:T(8,128)(2,1)S(1)} %fusion.45), channel_id=1, replica_groups=mesh['kv'=8,'tp'=4] {'kv'}, dimensions={0}, use_global_device_ids=true | all-gather | bytes 147456 | tf_op jit(solution)/shard_map/all_gather | solution.py:134
  210.5 0.2 convolution_convert_fusion.4
  210.8 10.3 %psum.53 = bf16[64,256]{1,0:T(8,128)(2,1)S(1)} all-reduce(bf16[64,256]{1,0:T(8,128)(2,1)S(1)} %convolution_convert_fusion.4), channel_id=1, replica_groups=mesh['kv'=8,'tp'=4] {'tp'}, use_global_device_ids=true, to_apply=%region_11.12 | all-reduce | flops 16384 | bytes 65536 | tf_op jit(solution)/shard_map/psum | solution.py:138
  221.1 1.1 convolution_convert_fusion
  222.3 0.1 fusion.32
  222.4 19.7 %psum.55 = bf16[64]{0:T(256)(128)(2,1)S(1)} all-reduce(bf16[64]{0:T(256)(128)(2,1)S(1)} %get-tuple-element.9), channel_id=1, replica_groups=mesh['kv'=8,'tp'=4] {'kv'}, use_global_device_ids=true, to_apply=%region_14.15 | all-reduce | flops 64 | bytes 256 | tf_op jit(solution)/shard_map/psum | solution.py:26
  242.1 51.1 %all-reduce.6.cloned.1.call-done = bf16[64,2816]{1,0:T(8,128)(2,1)} async-done(((bf16[64,2816]{1,0:T(8,128)(2,1)}), bf16[64,2816]{1,0:T(8,128)(2,1)}) %all-reduce.6.cloned.1.call-update) | async-done | bytes 360464 | tf_op jit(solution)/shard_map/psum | solution.py:25
  293.2 1.0 convert_element_type.117
  294.3 0.3 convolution_convert_fusion.3
  294.6 0.7 copy.37
  295.3 19.0 %reduce-scatter.7.cloned.1.call-done = bf16[64,64]{1,0:T(8,128)(2,1)} async-done(((bf16[256,64]{1,0:T(8,128)(2,1)}), bf16[64,64]{1,0:T(8,128)(2,1)}) %reduce-scatter.7.cloned.1.call-update) | async-done | bytes 8208
  314.3 0.8 copy.38
  315.1 0.7 add_convert_fusion
  (44 shorter events, 0.3 us)
Async XLA Ops:
  7.2 84.4 %copy-start = (bf16[1408,256]{1,0:T(8,128)(2,1)S(1)}, bf16[1408,256]{1,0:T(8,128)(2,1)}, u32[]{:S(2)}) copy-start(bf16[1408,256]{1,0:T(8,128)(2,1)} %param.26) | copy-start | bytes 2162692
  7.2 83.3 %all-reduce.4.cloned.1.call-start = ((), (), s32[]{:S(2)}) async-start(), calls=%async_computation.2 | async-start | bytes 720896 | tf_op jit(solution)/shard_map/psum | solution.py:25
  14.4 87.9 %copy-start.9 = (bf16[256,1024]{1,0:T(8,128)(2,1)S(1)}, bf16[256,1024]{1,0:T(8,128)(2,1)}, u32[]{:S(2)}) copy-start(bf16[256,1024]{1,0:T(8,128)(2,1)} %param.31) | copy-start | bytes 1572868
  14.4 87.9 %copy-start.10 = (bf16[256,1024]{1,0:T(8,128)(2,1)S(1)}, bf16[256,1024]{1,0:T(8,128)(2,1)}, u32[]{:S(2)}) copy-start(bf16[256,1024]{1,0:T(8,128)(2,1)} %param.30) | copy-start | bytes 1572868
  14.4 87.9 %copy-start.11 = (bf16[256,512]{1,0:T(8,128)(2,1)S(1)}, bf16[256,512]{1,0:T(8,128)(2,1)}, u32[]{:S(2)}) copy-start(bf16[256,512]{1,0:T(8,128)(2,1)} %param.29) | copy-start | bytes 786436
  14.4 87.9 %copy-start.12 = (bf16[256,512]{1,0:T(8,128)(2,1)S(1)}, bf16[256,512]{1,0:T(8,128)(2,1)}, u32[]{:S(2)}) copy-start(bf16[256,512]{1,0:T(8,128)(2,1)} %param.28) | copy-start | bytes 786436
  14.4 87.9 %copy-start.13 = (f32[256]{0:T(256)S(1)}, f32[256]{0:T(256)}, u32[]{:S(2)}) copy-start(f32[256]{0:T(256)} %param.27) | copy-start | bytes 3076
  17.0 148.2 %reduce-scatter.5.cloned.1.call-start = ((), (), s32[]{:S(2)}) async-start(), calls=%async_computation.3 | async-start | bytes 442368 | tf_op jit(solution)/shard_map/reduce_scatter | solution.py:95
  91.9 64.7 %copy-start.5 = (f32[8]{0:T(128)S(1)}, f32[8]{0:T(128)}, u32[]{:S(2)}) copy-start(f32[8]{0:T(128)} %param.35) | copy-start | bytes 100
  103.5 189.7 %all-reduce.6.cloned.1.call-start = ((), (), s32[]{:S(2)}) async-start(), calls=%async_computation.4 | async-start | bytes 720896 | tf_op jit(solution)/shard_map/psum | solution.py:25
  165.2 7.2 %copy-start.1 = (f32[8,8,128,128]{3,2,1,0:T(8,128)S(1)}, f32[8,8,128,128]{3,2,1,0:T(8,128)}, u32[]{:S(2)}) copy-start(f32[8,8,128,128]{3,2,1,0:T(8,128)} %param.22) | copy-start | bytes 12582916
  173.9 2.1 copy-start.2
  173.9 5.9 %copy-start.4 = (f32[128]{0:T(128)S(1)}, f32[128]{0:T(128)}, u32[]{:S(2)}) copy-start(f32[128]{0:T(128)} %param.36) | copy-start | bytes 1540
  173.9 36.6 %copy-start.3 = (bf16[1024,256]{1,0:T(8,128)(2,1)S(1)}, bf16[1024,256]{1,0:T(8,128)(2,1)}, u32[]{:S(2)}) copy-start(bf16[1024,256]{1,0:T(8,128)(2,1)} %param.37) | copy-start | bytes 1572868
  173.9 47.1 %copy-start.6 = (bf16[256,1408]{1,0:T(8,128)(2,1)S(1)}, bf16[256,1408]{1,0:T(8,128)(2,1)}, u32[]{:S(2)}) copy-start(bf16[256,1408]{1,0:T(8,128)(2,1)} %param.40) | copy-start | bytes 2162692
  174.0 47.1 %copy-start.7 = (bf16[256,1408]{1,0:T(8,128)(2,1)S(1)}, bf16[256,1408]{1,0:T(8,128)(2,1)}, u32[]{:S(2)}) copy-start(bf16[256,1408]{1,0:T(8,128)(2,1)} %param.39) | copy-start | bytes 2162692
  174.0 47.1 %copy-start.14 = (f32[256]{0:T(256)S(1)}, f32[256]{0:T(256)}, u32[]{:S(2)}) copy-start(f32[256]{0:T(256)} %param.38) | copy-start | bytes 3076
  179.7 114.5 %copy-start.8 = (bf16[1408,256]{1,0:T(8,128)(2,1)S(1)}, bf16[1408,256]{1,0:T(8,128)(2,1)}, u32[]{:S(2)}) copy-start(bf16[1408,256]{1,0:T(8,128)(2,1)} %param.41) | copy-start | bytes 2162692
  222.2 92.1 %reduce-scatter.7.cloned.1.call-start = ((), (), s32[]{:S(2)}) async-start(), calls=%async_computation.5 | async-start | bytes 81920
Sparse Core Ops, SparseCore 0:
  17.1 73.3 all-reduce.3
  103.6 61.5 reduce-scatter.4
  222.3 70.8 all-reduce.5
  295.5 18.7 reduce-scatter.6
where the time goes:
time: 323 us; the launch traced here: 322 us
  blocking collectives  152 us (47%)
  waiting for transfers between devices  126 us (39%)
  matrix products  15.2 us (5%)
  between operations  14.7 us (5%)
  other arithmetic  6.96 us (2%)
  local copies, waits for them, and re-layouts  6.68 us (2%)
    psum x2, waiting for transfers between devices, feed_forward(): lax.psum(partial_value.astype(jnp.bfloat16), 'kv').astype(jnp.float32)  98.7 us
    psum x2, blocking collectives, feed_forward(): lax.psum(squares.astype(jnp.bfloat16), 'kv').astype(jnp.float32)  42.1 us
    unnamed x1, blocking collectives  33.1 us
    all_gather x1, blocking collectives, token_mixer(): lax.all_gather(normed, 'kv', axis=0, tiled=True)  30.6 us
    psum x1, blocking collectives, token_mixer(): square_sums = lax.psum(squares, 'kv')  19.7 us
    unnamed x5, waiting for transfers between devices  19.1 us
    psum x1, blocking collectives, feed_forward(): branch = lax.psum(projected, 'tp').astype(jnp.float32)  10.3 us
    psum x1, blocking collectives, token_mixer(): branch = lax.psum(projected, 'tp').astype(jnp.float32)  10.3 us
  transfers between devices with their start and end apart: 4, of which 4 were waited for; matrix products, arithmetic and copies ran while one was open for 1% of the time, Pallas kernels for 0%

commit v1 on v0

--- a/solution.py
+++ b/solution.py
@@ -5,6 +5,10 @@
 
 D = 2048
 epsilon = 1e-06
+
+
+def order_boxes(block_here, axis_key):
+    return jax.lax.all_gather(block_here, axis_name=axis_key).sum(axis=0)
 
 
 def activate(summed, square_sums, hidden_cols):
@@ -22,7 +26,7 @@
     partial_value = jnp.dot(scaled, joined, preferred_element_type=jnp.float32)
     hidden_cols = gate_weight.shape[1]
     summed, square_sums = (
-        lax.psum(partial_value.astype(jnp.bfloat16), "kv").astype(jnp.float32),
+        order_boxes(partial_value.astype(jnp.bfloat16), "kv").astype(jnp.float32),
         lax.psum(squares.astype(jnp.bfloat16), "kv").astype(jnp.float32),
     )
     hidden = activate(summed, square_sums, hidden_cols)

time: 323 us -> 296 us (0.916)
  waiting for transfers between devices: 126 us -> 97.2 us
    psum x2 -> x0, waiting for transfers between devices: 98.7 us -> none  [feed_forward(): lax.psum(partial_value.astype(jnp.bfloat16), 'kv').astype(jnp.float32)]
    all_gather x0 -> x2, waiting for transfers between devices: none -> 70.4 us  [order_boxes(): return jax.lax.all_gather(block_here, axis_name=axis_key).sum(axis=0)]
    reduce_sum x0 -> x2, other arithmetic: none -> 4.59 us  [order_boxes(): return jax.lax.all_gather(block_here, axis_name=axis_key).sum(axis=0)]
where the time goes in v1:
time: 296 us; the launch traced here: 295 us
  blocking collectives  152 us (51%)
  waiting for transfers between devices  97.2 us (33%)
  matrix products  15.1 us (5%)
  between operations  14.7 us (5%)
  other arithmetic  9.58 us (3%)
  local copies, waits for them, and re-layouts  6.67 us (2%)
    all_gather x2, waiting for transfers between devices, order_boxes(): return jax.lax.all_gather(block_here, axis_name=axis_key).sum(axis=0)  70.4 us
    psum x2, blocking collectives, feed_forward(): lax.psum(squares.astype(jnp.bfloat16), 'kv').astype(jnp.float32)  42.3 us
    unnamed x1, blocking collectives  33.1 us
    all_gather x1, blocking collectives, token_mixer(): lax.all_gather(normed, 'kv', axis=0, tiled=True)  30.6 us
    psum x1, blocking collectives, token_mixer(): square_sums = lax.psum(squares, 'kv')  19.1 us
    unnamed x5, waiting for transfers between devices  18.4 us
    psum x1, blocking collectives, feed_forward(): branch = lax.psum(projected, 'tp').astype(jnp.float32)  10.3 us
    psum x1, blocking collectives, token_mixer(): branch = lax.psum(projected, 'tp').astype(jnp.float32)  10.3 us
  transfers between devices with their start and end apart: 4, of which 4 were waited for; matrix products, arithmetic and copies ran while one was open for 1% of the time, Pallas kernels for 0%

profile of v1, /device:TPU:0, one launch (start us, length us, event | category | flops | bytes accessed | tf_op | source)
XLA Modules:
  0.0 295.3 jit_solution(5119203935247764952)
XLA Ops:
  7.2 0.9 copy.27
  8.1 6.2 %all_gather.18 = bf16[64,256]{0,1:T(8,128)(2,1)S(1)} all-gather(bf16[64,64]{0,1:T(8,128)(2,1)S(1)} %copy.27), channel_id=1, replica_groups=mesh['kv'=8,'tp'=4] {'tp'}, dimensions={1}, use_global_device_ids=true | all-gather | bytes 40960 | tf_op jit(solution)/shard_map/all_gather | solution.py:169
  14.3 0.1 copy.28
  14.4 2.5 convolution_convert_fusion.2
  16.9 0.0 reduce-scatter.5.cloned.1.call-start
  16.9 1.2 dynamic-slice
  18.8 0.1 fusion.27
  18.9 22.5 %psum.35 = bf16[64]{0:T(256)(128)(2,1)S(1)} all-reduce(bf16[64]{0:T(256)(128)(2,1)S(1)} %fusion.27), channel_id=1, replica_groups=mesh['kv'=8,'tp'=4] {'kv'}, use_global_device_ids=true, to_apply=%region_2.0 | all-reduce | flops 64 | bytes 256 | tf_op jit(solution)/shard_map/psum | solution.py:30
  41.4 0.7 constant_dynamic-slice_fusion
  42.1 0.7 exponential_negate_fusion
  42.7 33.6 %all-gather.5.cloned.1.call-done = bf16[512,2816]{1,0:T(8,128)(2,1)} async-done(((bf16[64,2816]{1,0:T(8,128)(2,1)}), bf16[512,2816]{1,0:T(8,128)(2,1)}) %all-gather.5.cloned.1.call-update) | async-done | bytes 2883600 | tf_op jit(solution)/shard_map/all_gather | solution.py:11
  76.4 2.4 reduce_sum.78
  78.8 0.3 convolution_convert_fusion.5
  79.2 10.3 %psum.36 = bf16[64,256]{1,0:T(8,128)(2,1)S(1)} all-reduce(bf16[64,256]{1,0:T(8,128)(2,1)S(1)} %convolution_convert_fusion.5), channel_id=1, replica_groups=mesh['kv'=8,'tp'=4] {'tp'}, use_global_device_ids=true, to_apply=%region_3.4 | all-reduce | flops 16384 | bytes 65536 | tf_op jit(solution)/shard_map/psum | solution.py:45
  89.4 0.1 fusion.30
  89.6 1.1 convolution_convert_fusion.1
  90.8 19.1 %psum.37 = f32[64]{0:T(128)S(1)} all-reduce(f32[64]{0:T(128)S(1)} %get-tuple-element.4), channel_id=1, replica_groups=mesh['kv'=8,'tp'=4] {'kv'}, use_global_device_ids=true, to_apply=%region_6.7 | all-reduce | flops 64 | bytes 512 | tf_op jit(solution)/shard_map/psum | solution.py:94
  109.9 0.1 convolution_convert_fusion.6
  110.1 33.1 %all-reduce = bf16[64,16]{1,0:T(8,128)(2,1)S(1)} all-reduce(bf16[64,16]{1,0:T(8,128)(2,1)S(1)} %convolution_convert_fusion.6), channel_id=4, replica_groups=mesh['kv'=8,'tp'=4] {'kv'}, use_global_device_ids=true, to_apply=%region_4.5.clone | all-reduce | flops 1024 | bytes 4096
  143.1 0.1 add_rsqrt_fusion.4
  143.2 0.1 convert_multiply_fusion.5
  143.3 0.1 add_divide_fusion
  143.4 0.1 copy.30
  143.5 8.5 %reduce-scatter.5.cloned.1.call-done = bf16[8,3072]{1,0:T(8,128)(2,1)} async-done(((bf16[64,3072]{1,0:T(8,128)(2,1)}), bf16[8,3072]{1,0:T(8,128)(2,1)}) %reduce-scatter.5.cloned.1.call-update) | async-done | bytes 49168 | tf_op jit(solution)/shard_map/reduce_scatter | solution.py:99
  151.9 1.0 convert_multiply_fusion
  152.9 0.1 fusion.42
  153.1 0.1 fusion.43
  153.2 5.8 %fusion = f32[8,8,1,128]{3,2,1,0:T(1,128)S(1)} fusion(f32[8,8,128,1]{2,3,1,0:T(1,128)S(1)} %bitcast.61, f32[8,8,128,128]{3,2,1,0:T(8,128)} %param.22, f32[8,8]{1,0:T(8,128)S(1)} %get-tuple-element.11), kind=kOutput, calls=%fused_computation.1 | convolution fusion | flops 13631488 | bytes 4260096 | tf_op jit(solution)/shard_map/rhab,rha->rhb/dot_general | solution.py:56
  159.0 0.1 fusion.37
  159.1 1.5 multiply_add_fusion
  160.7 2.0 copy-done.2
  162.7 3.6 %fusion.59 = f32[8,8,1,128]{3,2,1,0:T(1,128)S(1)} fusion(f32[8,8,128,128]{3,2,1,0:T(8,128)S(1)} %multiply_add_fusion, f32[8,8,128,1]{2,3,1,0:T(1,128)S(1)} %bitcast.64), kind=kOutput, calls=%fused_computation.96 | convolution fusion | flops 12582912 | bytes 4259840 | tf_op jit(solution)/shard_map/rhab,rha->rhb/dot_general | solution.py:59
  166.4 0.1 fusion.35
  166.5 0.1 fusion.45
  166.6 30.6 %all_gather.21 = bf16[64,1024]{1,0:T(8,128)(2,1)S(1)} all-gather(bf16[8,1024]{1,0:T(8,128)(2,1)S(1)} %fusion.45), channel_id=1, replica_groups=mesh['kv'=8,'tp'=4] {'kv'}, dimensions={0}, use_global_device_ids=true | all-gather | bytes 147456 | tf_op jit(solution)/shard_map/all_gather | solution.py:138
  197.1 0.2 convolution_convert_fusion.4
  197.3 10.3 %psum.38 = bf16[64,256]{1,0:T(8,128)(2,1)S(1)} all-reduce(bf16[64,256]{1,0:T(8,128)(2,1)S(1)} %convolution_convert_fusion.4), channel_id=1, replica_groups=mesh['kv'=8,'tp'=4] {'tp'}, use_global_device_ids=true, to_apply=%region_11.12 | all-reduce | flops 16384 | bytes 65536 | tf_op jit(solution)/shard_map/psum | solution.py:142
  207.7 1.1 convolution_convert_fusion
  208.8 0.0 reduce-scatter.7.cloned.1.call-start
  208.9 0.1 fusion.32
  209.0 19.9 %psum.39 = bf16[64]{0:T(256)(128)(2,1)S(1)} all-reduce(bf16[64]{0:T(256)(128)(2,1)S(1)} %get-tuple-element.9), channel_id=1, replica_groups=mesh['kv'=8,'tp'=4] {'kv'}, use_global_device_ids=true, to_apply=%region_14.15 | all-reduce | flops 64 | bytes 256 | tf_op jit(solution)/shard_map/psum | solution.py:30
  228.9 36.7 %all-gather.7.cloned.1.call-done = bf16[512,2816]{1,0:T(8,128)(2,1)} async-done(((bf16[64,2816]{1,0:T(8,128)(2,1)}), bf16[512,2816]{1,0:T(8,128)(2,1)}) %all-gather.7.cloned.1.call-update) | async-done | bytes 2883600 | tf_op jit(solution)/shard_map/all_gather | solution.py:11
  265.6 2.2 reduce_sum.84
  267.9 0.3 convolution_convert_fusion.3
  268.2 0.7 copy.37
  268.9 18.3 %reduce-scatter.7.cloned.1.call-done = bf16[64,64]{1,0:T(8,128)(2,1)} async-done(((bf16[256,64]{1,0:T(8,128)(2,1)}), bf16[64,64]{1,0:T(8,128)(2,1)}) %reduce-scatter.7.cloned.1.call-update) | async-done | bytes 8208
  287.3 0.8 copy.38
  288.1 0.7 add_convert_fusion
  (46 shorter events, 0.4 us)
Async XLA Ops:
  7.2 71.7 %copy-start = (bf16[1408,256]{1,0:T(8,128)(2,1)S(1)}, bf16[1408,256]{1,0:T(8,128)(2,1)}, u32[]{:S(2)}) copy-start(bf16[1408,256]{1,0:T(8,128)(2,1)} %param.26) | copy-start | bytes 2162692
  7.2 69.2 %all-gather.5.cloned.1.call-start = ((), (), s32[]{:S(2)}) async-start(), calls=%async_computation.3 | async-start | bytes 3244032 | tf_op jit(solution)/shard_map/all_gather | solution.py:11
  16.9 135.1 %reduce-scatter.5.cloned.1.call-start = ((), (), s32[]{:S(2)}) async-start(), calls=%async_computation.2 | async-start | bytes 442368 | tf_op jit(solution)/shard_map/reduce_scatter | solution.py:99
  76.4 13.2 %copy-start.9 = (bf16[256,1024]{1,0:T(8,128)(2,1)S(1)}, bf16[256,1024]{1,0:T(8,128)(2,1)}, u32[]{:S(2)}) copy-start(bf16[256,1024]{1,0:T(8,128)(2,1)} %param.31) | copy-start | bytes 1572868
  76.4 13.2 %copy-start.10 = (bf16[256,1024]{1,0:T(8,128)(2,1)S(1)}, bf16[256,1024]{1,0:T(8,128)(2,1)}, u32[]{:S(2)}) copy-start(bf16[256,1024]{1,0:T(8,128)(2,1)} %param.30) | copy-start | bytes 1572868
  76.4 13.2 %copy-start.11 = (bf16[256,512]{1,0:T(8,128)(2,1)S(1)}, bf16[256,512]{1,0:T(8,128)(2,1)}, u32[]{:S(2)}) copy-start(bf16[256,512]{1,0:T(8,128)(2,1)} %param.29) | copy-start | bytes 786436
  76.4 13.2 %copy-start.12 = (bf16[256,512]{1,0:T(8,128)(2,1)S(1)}, bf16[256,512]{1,0:T(8,128)(2,1)}, u32[]{:S(2)}) copy-start(bf16[256,512]{1,0:T(8,128)(2,1)} %param.28) | copy-start | bytes 786436
  76.4 13.2 %copy-start.13 = (f32[256]{0:T(256)S(1)}, f32[256]{0:T(256)}, u32[]{:S(2)}) copy-start(f32[256]{0:T(256)} %param.27) | copy-start | bytes 3076
  79.1 64.1 %copy-start.5 = (f32[8]{0:T(128)S(1)}, f32[8]{0:T(128)}, u32[]{:S(2)}) copy-start(f32[8]{0:T(128)} %param.35) | copy-start | bytes 100
  90.8 174.8 %all-gather.7.cloned.1.call-start = ((), (), s32[]{:S(2)}) async-start(), calls=%async_computation.4 | async-start | bytes 3244032 | tf_op jit(solution)/shard_map/all_gather | solution.py:11
  151.9 7.2 %copy-start.1 = (f32[8,8,128,128]{3,2,1,0:T(8,128)S(1)}, f32[8,8,128,128]{3,2,1,0:T(8,128)}, u32[]{:S(2)}) copy-start(f32[8,8,128,128]{3,2,1,0:T(8,128)} %param.22) | copy-start | bytes 12582916
  160.6 2.1 copy-start.2
  160.6 5.9 %copy-start.4 = (f32[128]{0:T(128)S(1)}, f32[128]{0:T(128)}, u32[]{:S(2)}) copy-start(f32[128]{0:T(128)} %param.36) | copy-start | bytes 1540
  160.6 36.5 %copy-start.3 = (bf16[1024,256]{1,0:T(8,128)(2,1)S(1)}, bf16[1024,256]{1,0:T(8,128)(2,1)}, u32[]{:S(2)}) copy-start(bf16[1024,256]{1,0:T(8,128)(2,1)} %param.37) | copy-start | bytes 1572868
  160.6 47.0 %copy-start.6 = (bf16[256,1408]{1,0:T(8,128)(2,1)S(1)}, bf16[256,1408]{1,0:T(8,128)(2,1)}, u32[]{:S(2)}) copy-start(bf16[256,1408]{1,0:T(8,128)(2,1)} %param.40) | copy-start | bytes 2162692
  160.6 47.0 %copy-start.7 = (bf16[256,1408]{1,0:T(8,128)(2,1)S(1)}, bf16[256,1408]{1,0:T(8,128)(2,1)}, u32[]{:S(2)}) copy-start(bf16[256,1408]{1,0:T(8,128)(2,1)} %param.39) | copy-start | bytes 2162692
  160.6 47.0 %copy-start.14 = (f32[256]{0:T(256)S(1)}, f32[256]{0:T(256)}, u32[]{:S(2)}) copy-start(f32[256]{0:T(256)} %param.38) | copy-start | bytes 3076
  207.6 60.2 %copy-start.8 = (bf16[1408,256]{1,0:T(8,128)(2,1)S(1)}, bf16[1408,256]{1,0:T(8,128)(2,1)}, u32[]{:S(2)}) copy-start(bf16[1408,256]{1,0:T(8,128)(2,1)} %param.41) | copy-start | bytes 2162692
  208.8 78.5 %reduce-scatter.7.cloned.1.call-start = ((), (), s32[]{:S(2)}) async-start(), calls=%async_computation.5 | async-start | bytes 81920
Sparse Core Ops, SparseCore 0:
  17.0 59.3 all-gather.4
  90.9 60.9 reduce-scatter.4
  208.9 56.5 all-gather.6
  269.1 18.1 reduce-scatter.6
